TPU v7x, 512 devices: a whole 4x4x16 slice. The times are simulated.
512 devices in a mesh: ep: 128 (over z, x, core), tp: 4 (over y).
Axes of the slice: x: 4, y: 4, z: 16, core: 2. Of those that a mesh axis runs over, the one named last changes fastest.
Arguments:
- tokens: bfloat16 [512, 2048], P('ep', 'tp'), may hold values from -6 to 6
- norm_gain: bfloat16 [2048], P('tp'), may hold values from 0.099609375 to 1.8984375
- w_query: bfloat16 [2048, 2048], P('tp', 'ep'), may hold values from -0.125 to 0.125
- w_forget: bfloat16 [2048, 2048], P('tp', 'ep'), may hold values from -0.125 to 0.125
- w_input: bfloat16 [2048, 2048], P('tp', 'ep'), may hold values from -0.125 to 0.125
- forget_floor: float32 [2048], P('tp'), may hold values from 0 to 0.9
- head_gain: bfloat16 [128], replicated, may hold values from 0.099609375 to 1.8984375
- w_output: bfloat16 [2048, 2048], P('tp', 'ep'), may hold values from -0.125 to 0.125
- state: float32 [512, 16, 128, 128], P('ep', 'tp'), may hold values from -6 to 6
- ffn_gain: bfloat16 [2048], P('tp'), may hold values from 0.099609375 to 1.8984375
- route_experts: int32 [512, 2], P('ep'), may hold values from 0 to 7, all different within a row; in each aligned block of 4 rows (0 to 3, 4 to 7, ...) at most 2 rows name the same one
- route_weights: float32 [512, 2], P('ep'), may hold values from 0.1 to 1
- w_gate: bfloat16 [128, 2048, 448], P('ep', None, 'tp'), may hold values from -0.125 to 0.125
- w_up: bfloat16 [128, 2048, 448], P('ep', None, 'tp'), may hold values from -0.125 to 0.125
- w_down: bfloat16 [128, 448, 2048], P('ep', 'tp'), may hold values from -0.0625 to 0.0625
Outputs:
- mixed: bfloat16 [512, 2048], P('ep', 'tp')
- new_state: float32 [512, 16, 128, 128], P('ep', 'tp')
Inputs may be any that keep to these rules, and one draw needn't show every extreme that they name: `route_experts`: each row names two different experts. Among the rows of one index of ep, no expert is named by more than 2 rows, and in every draw some expert is named by exactly 2 of them.
All inputs are finite; a program needn't handle non-finite values.
Results may differ from a plain program's by a relative error of at most 0.014.
Values may be sent and summed in bfloat16 or wider, within the bound.
No kernel may reach another device: no remote copies, remote signals or barrier semaphores. Data moves between devices by JAX's collectives and lax.ppermute only.
A program may use at most 64 MiB of HBM per device.

v0:
```python
import jax
import jax.numpy as jnp
from jax import lax
from jax.sharding import Mesh
from jax.sharding import PartitionSpec as P

EXPERTS = 8
EP = ("ep_0", "ep_1", "ep_2")
EPS = 1e-06


def laid_out(blocks, dim):
    blocks = jnp.moveaxis(blocks, 0, dim)
    dims = blocks.shape
    return blocks.reshape(*dims[:dim], dims[dim] * dims[dim + 1], *dims[dim + 2 :])


def all_blocks(shard, axes, sequence):
    blocks = shard
    for k in sequence:
        blocks = lax.all_gather(blocks, axes[k])
    done = sequence[::-1]
    back = [done.index(k) for k in range(len(axes))]
    blocks = blocks.transpose(*back, *range(len(axes), blocks.ndim))
    return blocks.reshape(-1, *shard.shape)


def whole_of(shard, axes, sequence, dim):
    return laid_out(all_blocks(shard, axes, sequence), dim)


def in_blocks(shard, dim, length):
    before, after = (shard.shape[:dim], shard.shape[dim + 1 :])
    return jnp.moveaxis(shard.reshape(*before, length, -1, *after), dim, 0)


def sent_and_summed(shard, axis, dim):
    length = lax.axis_size(axis)
    blocks = lax.all_to_all(in_blocks(shard, dim, length), axis, 0, 0, tiled=True)
    return jnp.sum(blocks, axis=0)


def summed_on_arrival(shard, axis, dim):
    blocks = in_blocks(shard, dim, lax.axis_size(axis))
    arrived = lax.all_to_all(blocks, axis, split_axis=0, concat_axis=0, tiled=True)
    return arrived.astype(jnp.float32).sum(axis=0)


def shards(
    tokens,
    norm_gain,
    w_query,
    w_forget,
    w_input,
    forget_floor,
    head_gain,
    w_output,
    state,
    ffn_gain,
    route_experts,
    route_weights,
    w_gate,
    w_up,
    w_down,
):
    ep_count = lax.axis_size(EP)
    tp_count = lax.axis_size("tp")
    seq_count = tokens.shape[0]
    model_width = tokens.shape[1] * tp_count
    head_size = state.shape[2]
    local_heads = state.shape[1]
    tok_f32 = tokens.astype(jnp.float32)
    sum_sq = lax.psum(jnp.sum(tok_f32 * tok_f32, axis=1), "tp")
    normed = (
        tok_f32 * lax.rsqrt(sum_sq / model_width + EPS)[:, None] * norm_gain.astype(jnp.float32)
    ).astype(jnp.bfloat16)
    w_joint = jnp.concatenate([w_query, w_forget, w_input], axis=1)
    partial_value = jnp.dot(
        whole_of(normed, EP, (1, 0, 2), 0), w_joint, preferred_element_type=jnp.float32
    )
    moved_in = lax.all_to_all(partial_value, EP, split_axis=0, concat_axis=1, tiled=True)
    summed = sent_and_summed(moved_in, "tp", 1)
    col_count = w_query.shape[1]
    blocks = summed.reshape(seq_count, -1, 3, col_count)
    queries = blocks[:, :, 0, :].reshape(seq_count, local_heads, head_size)
    fgate = blocks[:, :, 1, :].reshape(seq_count, local_heads, head_size)
    inputs = blocks[:, :, 2, :].reshape(seq_count, local_heads, head_size)
    floors = forget_floor.reshape(local_heads, head_size)
    forget = floors + (1.0 - floors) * jax.nn.sigmoid(fgate)
    new_state = forget[..., None] * state + (1.0 - forget)[..., None] * inputs[:, :, None, :]
    reads = jnp.einsum(
        "bhk,bhkv->bhv", jax.nn.silu(queries), new_state, precision=lax.Precision.HIGHEST
    )
    head_sq = jnp.mean(reads * reads, axis=-1, keepdims=True)
    heads_out = (
        (reads * lax.rsqrt(head_sq + EPS) * head_gain.astype(jnp.float32))
        .reshape(seq_count, local_heads * head_size)
        .astype(jnp.bfloat16)
    )
    part_out = jnp.dot(
        whole_of(heads_out, EP, (1, 0, 2), 0), w_output, preferred_element_type=jnp.float32
    )
    moved_out = lax.all_to_all(
        part_out.astype(jnp.bfloat16), EP, split_axis=0, concat_axis=1, tiled=True
    ).astype(part_out.dtype)
    mixer_slice = summed_on_arrival(moved_out.astype(jnp.bfloat16), "tp", 1).astype(jnp.bfloat16)
    middle = (tok_f32 + mixer_slice.astype(jnp.float32)).astype(jnp.bfloat16)
    middle_f32 = middle.astype(jnp.float32)
    span_count = ep_count // EXPERTS
    capacity = max(2, seq_count // 2)
    positions = jnp.arange(seq_count, dtype=jnp.int32)
    earlier = positions[None, :] < positions[:, None]
    same_expert = route_experts[:, :, None, None] == route_experts[None, None, :, :]
    slot_rank = jnp.sum(same_expert & earlier[:, None, :, None], axis=(2, 3))
    owners = jnp.arange(ep_count, dtype=jnp.int32) // span_count
    matched = route_experts[None, :, :] == owners[:, None, None]
    placed = slot_rank[:, :, None] == jnp.arange(capacity, dtype=jnp.int32)[None, None, :]
    slot_hits = matched[:, :, :, None] & placed[None, :, :, :]
    chosen = jnp.sum(slot_hits.astype(jnp.float32), axis=2).astype(jnp.bfloat16)
    weight_hits = jnp.sum(slot_hits.astype(jnp.float32) * route_weights[None, :, :, None], axis=2)
    row_stat = lax.psum(jnp.sum(middle_f32 * middle_f32, axis=1), "tp")
    second = (
        middle_f32 * lax.rsqrt(row_stat / model_width + EPS)[:, None] * ffn_gain.astype(jnp.float32)
    ).astype(jnp.bfloat16)
    outgoing = jnp.einsum("pts,td->psd", chosen, second, preferred_element_type=jnp.float32).astype(
        jnp.bfloat16
    )
    arrived_part = lax.all_to_all(outgoing, EP, split_axis=0, concat_axis=0, tiled=True)
    arrived = lax.all_gather(arrived_part, "tp", axis=2, tiled=True)
    expert_rows = arrived.reshape(ep_count * capacity, model_width)
    gate_act = jnp.dot(expert_rows, w_gate[0], preferred_element_type=jnp.float32)
    up_act = jnp.dot(expert_rows, w_up[0], preferred_element_type=jnp.float32)
    hidden = (jax.nn.silu(gate_act) * up_act).astype(jnp.bfloat16)
    piece_out = jnp.dot(hidden, w_down[0], preferred_element_type=jnp.float32)
    piece_total = summed_on_arrival(piece_out.astype(jnp.bfloat16), "tp", 1)
    returned = lax.all_to_all(
        piece_total.reshape(ep_count, capacity, -1).astype(jnp.bfloat16),
        EP,
        split_axis=0,
        concat_axis=0,
        tiled=True,
    ).astype(jnp.float32)
    routed = jnp.einsum("pts,psd->td", weight_hits, returned, precision=lax.Precision.HIGHEST)
    result = (middle_f32 + routed).astype(jnp.bfloat16)
    return (result, new_state)


def solution(mesh):
    torus = Mesh(mesh.devices.reshape(16, 4, 2, mesh.shape["tp"]), ("ep_0", "ep_1", "ep_2", "tp"))
    in_specs = (
        P(EP, "tp"),
        P("tp"),
        P("tp", EP),
        P("tp", EP),
        P("tp", EP),
        P("tp"),
        P(),
        P("tp", EP),
        P(EP, "tp", None, None),
        P("tp"),
        P(EP, None),
        P(EP, None),
        P(EP, None, "tp"),
        P(EP, None, "tp"),
        P(EP, "tp", None),
    )
    out_specs = (P(EP, "tp"), P(EP, "tp", None, None))
    return jax.shard_map(
        shards, mesh=torus, in_specs=in_specs, out_specs=out_specs, check_vma=False
    )
```

profile of v0, /device:TPU:33, one launch (start us, length us, event | category | flops | bytes accessed | tf_op | source)
XLA Modules:
  0.0 324.9 jit_solution(1485527307813868062)
XLA Ops:
  7.2 0.9 fusion.22
  8.0 8.7 %psum.14 = f32[4]{0:T(128)S(1)} all-reduce(f32[4]{0:T(128)S(1)} %fusion.22), channel_id=1, replica_groups=mesh['ep_0'=16,'ep_1'=4,'ep_2'=2,'tp'=4] {'tp'}, use_global_device_ids=true, to_apply=%region_1.0 | all-reduce | flops 4 | bytes 32 | tf_op jit(solution)/shard_map/psum | solution.py:73
  16.8 0.7 convert_element_type.76
  17.5 0.8 fusion.31
  18.2 9.5 %all-gather.5 = bf16[4,4,512]{2,1,0:T(4,128)(2,1)S(1)} all-gather(bf16[1,4,512]{2,1,0:T(4,128)(2,1)S(1)} %fusion.31), channel_id=2, replica_groups=mesh['ep_0'=16,'ep_1'=4,'ep_2'=2,'tp'=4] {'ep_1'}, dimensions={0}, use_global_device_ids=true | all-gather | bytes 20480 | tf_op jit(solution)/shard_map/all_gather | solution.py:21
  27.7 27.8 %all-gather.1 = bf16[64,4,512]{2,1,0:T(4,128)(2,1)S(1)} all-gather(bf16[4,4,512]{2,1,0:T(4,128)(2,1)S(1)} %all-gather.5), channel_id=3, replica_groups=mesh['ep_0'=16,'ep_1'=4,'ep_2'=2,'tp'=4] {'ep_0'}, dimensions={0}, use_global_device_ids=true | all-gather | bytes 278528 | tf_op jit(solution)/shard_map/all_gather | solution.py:21
  55.4 14.3 %all-gather.2 = bf16[32,4,4,512]{3,2,1,0:T(4,128)(2,1)S(1)} all-gather(bf16[16,4,4,512]{3,2,1,0:T(4,128)(2,1)S(1)} %bitcast.70), channel_id=4, replica_groups=mesh['ep_0'=16,'ep_1'=4,'ep_2'=2,'tp'=4] {'ep_2'}, dimensions={0}, use_global_device_ids=true | all-gather | bytes 786432 | tf_op jit(solution)/shard_map/all_gather | solution.py:21
  71.3 1.0 reshape.148
  72.2 12.0 %all-to-all-start = ((f32[128,1,192]{2,1,0:T(1,128)}), f32[128,1,192]{2,1,0:T(1,128)S(1)}, u32[]{:S(2)}, u32[]{:S(2)}) async-start(f32[128,1,192]{2,1,0:T(1,128)} %reshape.148), calls=%async_computation | async-start | bytes 262144 | tf_op jit(solution)/shard_map/all_to_all | solution.py:81
  84.4 17.0 %all-to-all-done = f32[128,1,192]{2,1,0:T(1,128)S(1)} async-done(((f32[128,1,192]{2,1,0:T(1,128)}), f32[128,1,192]{2,1,0:T(1,128)S(1)}, u32[]{:S(2)}, u32[]{:S(2)}) %all-to-all-start) | async-done | bytes 98336 | tf_op jit(solution)/shard_map/all_to_all | solution.py:81
  101.9 1.0 reduce.10
  103.3 0.7 copy.124
  103.9 3.3 %all-to-all-start.1 = ((f32[4,4,1536]{2,1,0:T(4,128)}), f32[4,4,1536]{2,1,0:T(4,128)S(1)}, u32[]{:S(2)}, u32[]{:S(2)}) async-start(f32[4,4,1536]{2,1,0:T(4,128)} %copy.124), calls=%async_computation.1 | async-start | bytes 196608 | tf_op jit(solution)/shard_map/all_to_all | solution.py:39
  107.5 4.4 %all-to-all-done.1 = f32[4,4,1536]{2,1,0:T(4,128)S(1)} async-done(((f32[4,4,1536]{2,1,0:T(4,128)}), f32[4,4,1536]{2,1,0:T(4,128)S(1)}, u32[]{:S(2)}, u32[]{:S(2)}) %all-to-all-start.1) | async-done | bytes 98336 | tf_op jit(solution)/shard_map/all_to_all | solution.py:39
  113.6 1.0 copy-done.1
  114.6 1.0 fusion.38
  115.8 9.1 %all_gather.43 = bf16[4,4,512]{2,1,0:T(4,128)(2,1)S(1)} all-gather(bf16[1,4,512]{2,1,0:T(4,128)(2,1)S(1)} %convert_element_type.80), channel_id=1, replica_groups=mesh['ep_0'=16,'ep_1'=4,'ep_2'=2,'tp'=4] {'ep_1'}, dimensions={0}, use_global_device_ids=true | all-gather | bytes 20480 | tf_op jit(solution)/shard_map/all_gather | solution.py:21
  124.9 20.2 %all-gather.3 = bf16[64,4,512]{2,1,0:T(4,128)(2,1)S(1)} all-gather(bf16[4,4,512]{2,1,0:T(4,128)(2,1)S(1)} %all_gather.43), channel_id=5, replica_groups=mesh['ep_0'=16,'ep_1'=4,'ep_2'=2,'tp'=4] {'ep_0'}, dimensions={0}, use_global_device_ids=true | all-gather | bytes 278528 | tf_op jit(solution)/shard_map/all_gather | solution.py:21
  145.1 13.3 %all-gather.4 = bf16[32,4,4,512]{3,2,1,0:T(4,128)(2,1)S(1)} all-gather(bf16[16,4,4,512]{3,2,1,0:T(4,128)(2,1)S(1)} %bitcast.71), channel_id=6, replica_groups=mesh['ep_0'=16,'ep_1'=4,'ep_2'=2,'tp'=4] {'ep_2'}, dimensions={0}, use_global_device_ids=true | all-gather | bytes 786432 | tf_op jit(solution)/shard_map/all_gather | solution.py:21
  159.7 0.8 copy.129
  160.4 9.0 %all-to-all-start.2 = ((bf16[128,4,16]{2,1,0:T(4,128)(2,1)}), bf16[128,4,16]{2,1,0:T(4,128)(2,1)S(1)}, u32[]{:S(2)}, u32[]{:S(2)}) async-start(bf16[128,4,16]{2,1,0:T(4,128)(2,1)} %bitcast.15), calls=%async_computation.2 | async-start | bytes 262144 | tf_op jit(solution)/shard_map/all_to_all | solution.py:103
  169.5 17.1 %all-to-all-done.2 = bf16[128,4,16]{2,1,0:T(4,128)(2,1)S(1)} async-done(((bf16[128,4,16]{2,1,0:T(4,128)(2,1)}), bf16[128,4,16]{2,1,0:T(4,128)(2,1)S(1)}, u32[]{:S(2)}, u32[]{:S(2)}) %all-to-all-start.2) | async-done | bytes 16416 | tf_op jit(solution)/shard_map/all_to_all | solution.py:103
  187.3 3.2 all-to-all-start.3
  190.7 4.0 %all-to-all-done.3 = bf16[4,4,512]{2,1,0:T(4,128)(2,1)S(1)} async-done(((bf16[4,4,512]{2,1,0:T(4,128)(2,1)}), bf16[4,4,512]{2,1,0:T(4,128)(2,1)S(1)}, u32[]{:S(2)}, u32[]{:S(2)}) %all-to-all-start.3) | async-done | bytes 16416 | tf_op jit(solution)/shard_map/all_to_all | solution.py:45
  194.9 6.9 %psum.15 = f32[4]{0:T(128)S(1)} all-reduce(f32[4]{0:T(128)S(1)} %fusion.26), channel_id=1, replica_groups=mesh['ep_0'=16,'ep_1'=4,'ep_2'=2,'tp'=4] {'tp'}, use_global_device_ids=true, to_apply=%region_9.10 | all-reduce | flops 4 | bytes 32 | tf_op jit(solution)/shard_map/psum | solution.py:121
  202.4 31.9 %all_to_all.54 = bf16[128,2,512]{2,1,0:T(2,128)(2,1)} all-to-all(bf16[128,2,512]{2,1,0:T(2,128)(2,1)S(1)} %copy.132), channel_id=1, replica_groups=mesh['ep_0'=16,'ep_1'=4,'ep_2'=2,'tp'=4] {'ep_0','ep_1','ep_2'}, dimensions={0} | all-to-all | bytes 524288 | tf_op jit(solution)/shard_map/all_to_all | solution.py:128
  234.4 20.6 %all-gather.8.cloned.1.call-done = bf16[128,2,2048]{2,1,0:T(2,128)(2,1)} async-done(((bf16[128,2,512]{2,1,0:T(2,128)(2,1)}), bf16[128,2,2048]{2,1,0:T(2,128)(2,1)}) %all-gather.8.cloned.1.call-update) | async-done | bytes 1048592 | tf_op jit(solution)/shard_map/all_gather | solution.py:129
  255.0 1.5 reshape.121
  257.5 1.4 convolution_convert_fusion
  259.0 16.2 %all_to_all.55 = bf16[4,256,512]{2,1,0:T(8,128)(2,1)S(1)} all-to-all(bf16[4,256,512]{2,1,0:T(8,128)(2,1)S(1)} %bitcast.67), channel_id=1, replica_groups=mesh['ep_0'=16,'ep_1'=4,'ep_2'=2,'tp'=4] {'tp'}, dimensions={0} | all-to-all | bytes 2097152 | tf_op jit(solution)/shard_map/all_to_all | solution.py:45
  275.5 41.7 %all_to_all.56 = bf16[128,2,512]{2,1,0:T(2,128)(2,1)S(1)} all-to-all(bf16[128,2,512]{2,1,0:T(2,128)(2,1)S(1)} %convert_element_type.93), channel_id=1, replica_groups=mesh['ep_0'=16,'ep_1'=4,'ep_2'=2,'tp'=4] {'ep_0','ep_1','ep_2'}, dimensions={0} | all-to-all | bytes 524288 | tf_op jit(solution)/shard_map/all_to_all | solution.py:136
  317.2 0.8 fusion.2
  (82 shorter events, 8.9 us)
Async XLA Ops:
  7.2 249.8 %copy-start = (bf16[1,112,2048]{2,1,0:T(8,128)(2,1)S(1)}, bf16[1,112,2048]{2,1,0:T(8,128)(2,1)}, u32[]{:S(2)}) copy-start(bf16[1,112,2048]{2,1,0:T(8,128)(2,1)} %param.29) | copy-start | bytes 1376260
  70.0 0.8 copy-start.7
  70.0 0.8 copy-start.8
  70.0 0.8 copy-start.9
  70.8 13.4 %copy-start.10 = (s32[4,2]{0,1:T(2,128)S(1)}, s32[4,2]{0,1:T(2,128)}, u32[]{:S(2)}) copy-start(s32[4,2]{0,1:T(2,128)} %param.25) | copy-start | bytes 100
  70.8 13.5 %copy-start.14 = (bf16[128]{0:T(256)(128)(2,1)S(1)}, bf16[128]{0:T(256)(128)(2,1)}, u32[]{:S(2)}) copy-start(bf16[128]{0:T(256)(128)(2,1)} %param.21) | copy-start | bytes 772
  70.9 13.5 %copy-start.11 = (f32[512]{0:T(512)S(1)}, f32[512]{0:T(512)}, u32[]{:S(2)}) copy-start(f32[512]{0:T(512)} %param.20) | copy-start | bytes 6148
  72.2 29.1 %all-to-all-start = ((f32[128,1,192]{2,1,0:T(1,128)}), f32[128,1,192]{2,1,0:T(1,128)S(1)}, u32[]{:S(2)}, u32[]{:S(2)}) async-start(f32[128,1,192]{2,1,0:T(1,128)} %reshape.148), calls=%async_computation | async-start | bytes 262144 | tf_op jit(solution)/shard_map/all_to_all | solution.py:81
  103.0 10.0 %copy-start.2 = (f32[4,4,128,128]{3,2,1,0:T(8,128)S(1)}, f32[4,4,128,128]{3,2,1,0:T(8,128)}, u32[]{:S(2)}) copy-start(f32[4,4,128,128]{3,2,1,0:T(8,128)} %param.23) | copy-start | bytes 3145732
  103.9 7.9 %all-to-all-start.1 = ((f32[4,4,1536]{2,1,0:T(4,128)}), f32[4,4,1536]{2,1,0:T(4,128)S(1)}, u32[]{:S(2)}, u32[]{:S(2)}) async-start(f32[4,4,1536]{2,1,0:T(4,128)} %copy.124), calls=%async_computation.1 | async-start | bytes 196608 | tf_op jit(solution)/shard_map/all_to_all | solution.py:39
  113.6 1.0 copy-start.1
  158.7 0.7 copy-start.6
  159.1 31.5 %copy-start.12 = (f32[4,2]{0,1:T(2,128)S(1)}, f32[4,2]{0,1:T(2,128)}, u32[]{:S(2)}) copy-start(f32[4,2]{0,1:T(2,128)} %param.26) | copy-start | bytes 100
  159.1 35.6 %copy-start.5 = (bf16[4,512]{1,0:T(4,128)(2,1)S(1)}, bf16[4,512]{1,0:T(4,128)(2,1)}, u32[]{:S(2)}) copy-start(bf16[4,512]{1,0:T(4,128)(2,1)} %param.15) | copy-start | bytes 12292
  159.2 35.8 %copy-start.13 = (bf16[512]{0:T(512)(128)(2,1)S(1)}, bf16[512]{0:T(512)(128)(2,1)}, u32[]{:S(2)}) copy-start(bf16[512]{0:T(512)(128)(2,1)} %param.24) | copy-start | bytes 3076
  160.4 26.1 %all-to-all-start.2 = ((bf16[128,4,16]{2,1,0:T(4,128)(2,1)}), bf16[128,4,16]{2,1,0:T(4,128)(2,1)S(1)}, u32[]{:S(2)}, u32[]{:S(2)}) async-start(bf16[128,4,16]{2,1,0:T(4,128)(2,1)} %bitcast.15), calls=%async_computation.2 | async-start | bytes 262144 | tf_op jit(solution)/shard_map/all_to_all | solution.py:103
  187.3 7.4 %all-to-all-start.3 = ((bf16[4,4,512]{2,1,0:T(4,128)(2,1)}), bf16[4,4,512]{2,1,0:T(4,128)(2,1)S(1)}, u32[]{:S(2)}, u32[]{:S(2)}) async-start(bf16[4,4,512]{2,1,0:T(4,128)(2,1)} %copy.131), calls=%async_computation.3 | async-start | bytes 32768 | tf_op jit(solution)/shard_map/all_to_all | solution.py:45
  190.6 64.4 %all-gather.8.cloned.1.call-start = ((), (), s32[]{:S(2)}) async-start(), calls=%async_computation.7 | async-start | bytes 1310720 | tf_op jit(solution)/shard_map/all_gather | solution.py:129
  234.4 22.1 %copy-start.4 = (bf16[1,2048,112]{1,2,0:T(8,128)(2,1)S(1)}, bf16[1,2048,112]{1,2,0:T(8,128)(2,1)}, u32[]{:S(2)}) copy-start(bf16[1,2048,112]{1,2,0:T(8,128)(2,1)} %param.27) | copy-start | bytes 1376260
  256.4 1.0 copy-start.3
Sparse Core Ops, SparseCore 0:
  234.5 20.4 all-gather.7
where the time goes:
time: 326 us; the launch traced here: 325 us
  blocking collectives  200 us (61%)
  waiting for transfers between devices  63.1 us (19%)
  starting transfers between devices  27.6 us (8%)
  between operations  14.5 us (4%)
  local copies, waits for them, and re-layouts  10.8 us (3%)
  other arithmetic  4.91 us (2%)
  matrix products  4.43 us (1%)
    all_gather x6, blocking collectives, all_blocks(): blocks = lax.all_gather(blocks, axes[k])  94.2 us
    all_to_all x1, blocking collectives, shards(): lax.all_to_all(piece_total.reshape(ep_count, capacity, -1).astype(jnp.bfl...  41.7 us
    all_to_all x1, blocking collectives, shards(): lax.all_to_all(outgoing, EP, split_axis=0, concat_axis=0, tiled=True)  31.9 us
    all_gather x1, waiting for transfers between devices, shards(): arrived = lax.all_gather(arrived_part, 'tp', axis=2, tiled=True)  20.6 us
    all_to_all x1, waiting for transfers between devices, shards(): lax.all_to_all(part_out.astype(jnp.bfloat16), EP, split_axis=0, concat_ax...  17.1 us
    all_to_all x1, waiting for transfers between devices, shards(): lax.all_to_all(partial_value, EP, split_axis=0, concat_axis=1, tiled=True)  17 us
    all_to_all x1, blocking collectives, summed_on_arrival(): lax.all_to_all(blocks, axis, split_axis=0, concat_axis=0, tiled=True)  16.2 us
    all_to_all x1, starting transfers between devices, shards(): lax.all_to_all(partial_value, EP, split_axis=0, concat_axis=1, tiled=True)  12 us
  transfers between devices with their start and end apart: 5, of which 5 were waited for; matrix products, arithmetic and copies ran while one was open for 0% of the time, Pallas kernels for 0%

commit v1 on v0

--- a/solution.py
+++ b/solution.py
@@ -7,6 +7,14 @@
 EXPERTS = 8
 EP = ("ep_0", "ep_1", "ep_2")
 EPS = 1e-06
+
+
+def gather_from_all(shard, axis, dim):
+    size = lax.axis_size(axis)
+    repeats = [size if d == dim else 1 for d in range(shard.ndim)]
+    return lax.all_to_all(
+        jnp.tile(shard, repeats), axis, split_axis=dim, concat_axis=dim, tiled=True
+    )
 
 
 def laid_out(blocks, dim):
@@ -126,7 +134,7 @@
         jnp.bfloat16
     )
     arrived_part = lax.all_to_all(outgoing, EP, split_axis=0, concat_axis=0, tiled=True)
-    arrived = lax.all_gather(arrived_part, "tp", axis=2, tiled=True)
+    arrived = gather_from_all(arrived_part, "tp", 2)
     expert_rows = arrived.reshape(ep_count * capacity, model_width)
     gate_act = jnp.dot(expert_rows, w_gate[0], preferred_element_type=jnp.float32)
     up_act = jnp.dot(expert_rows, w_up[0], preferred_element_type=jnp.float32)

time: 326 us -> 301 us (0.923)
  waiting for transfers between devices: 63.1 us -> 42.5 us
  between operations: 14.5 us -> 1.12 us
  blocking collectives: 200 us -> 205 us
    all_gather x1 -> x0, waiting for transfers between devices: 20.6 us -> none  [shards(): arrived = lax.all_gather(arrived_part, 'tp', axis=2, tiled=True)]
    all_to_all x0 -> x1, blocking collectives: none -> 17.3 us  [gather_from_all(): lax.all_to_all(jnp.tile(shard, repeats), axis, split_axis=dim, concat_axi...]
    all_to_all x1, blocking collectives: 41.7 us -> 29.9 us  [shards(): lax.all_to_all(piece_total.reshape(ep_count, capacity, -1).astype(jnp.bfl...]
    all_to_all x0 -> x2, local copies, waits for them, and re-layouts: none -> 3.4 us  [the longest x1 3.01 us: gather_from_all(): lax.all_to_all(jnp.tile(shard, repeats), axis, split_axis=dim, concat_axi...]
  transfers between devices with their start and end apart: 5 -> 4, of which waited for: 5 -> 4; matrix products, arithmetic and copies ran while one was open for 0% -> 0% of each run, Pallas kernels for 0% -> 0%
where the time goes in v1:
time: 301 us; the launch traced here: 300 us
  blocking collectives  205 us (68%)
  waiting for transfers between devices  42.5 us (14%)
  starting transfers between devices  27.6 us (9%)
  local copies, waits for them, and re-layouts  13.2 us (4%)
  matrix products  5.51 us (2%)
  other arithmetic  4.91 us (2%)
    all_gather x6, blocking collectives, all_blocks(): blocks = lax.all_gather(blocks, axes[k])  94.2 us
    all_to_all x1, blocking collectives, shards(): lax.all_to_all(outgoing, EP, split_axis=0, concat_axis=0, tiled=True)  31.8 us
    all_to_all x1, blocking collectives, shards(): lax.all_to_all(piece_total.reshape(ep_count, capacity, -1).astype(jnp.bfl...  29.9 us
    all_to_all x1, blocking collectives, gather_from_all(): lax.all_to_all(jnp.tile(shard, repeats), axis, split_axis=dim, concat_axi...  17.3 us
    all_to_all x1, waiting for transfers between devices, shards(): lax.all_to_all(part_out.astype(jnp.bfloat16), EP, split_axis=0, concat_ax...  17.1 us
    all_to_all x1, waiting for transfers between devices, shards(): lax.all_to_all(partial_value, EP, split_axis=0, concat_axis=1, tiled=True)  17 us
    all_to_all x1, blocking collectives, summed_on_arrival(): lax.all_to_all(blocks, axis, split_axis=0, concat_axis=0, tiled=True)  16.4 us
    all_to_all x1, starting transfers between devices, shards(): lax.all_to_all(partial_value, EP, split_axis=0, concat_axis=1, tiled=True)  12 us
  transfers between devices with their start and end apart: 4, of which 4 were waited for; matrix products, arithmetic and copies ran while one was open for 0% of the time, Pallas kernels for 0%

profile of v1, /device:TPU:33, one launch (start us, length us, event | category | flops | bytes accessed | tf_op | source)
XLA Modules:
  0.0 300.0 jit_solution(13555992844682213496)
XLA Ops:
  0.6 0.9 fusion.22
  1.5 8.7 %psum.14 = f32[4]{0:T(128)S(1)} all-reduce(f32[4]{0:T(128)S(1)} %fusion.22), channel_id=1, replica_groups=mesh['ep_0'=16,'ep_1'=4,'ep_2'=2,'tp'=4] {'tp'}, use_global_device_ids=true, to_apply=%region_1.0 | all-reduce | flops 4 | bytes 32 | tf_op jit(solution)/shard_map/psum | solution.py:81
  10.2 0.7 convert_element_type.76
  10.9 0.8 fusion.31
  11.7 9.5 %all-gather.5 = bf16[4,4,512]{2,1,0:T(4,128)(2,1)S(1)} all-gather(bf16[1,4,512]{2,1,0:T(4,128)(2,1)S(1)} %fusion.31), channel_id=2, replica_groups=mesh['ep_0'=16,'ep_1'=4,'ep_2'=2,'tp'=4] {'ep_1'}, dimensions={0}, use_global_device_ids=true | all-gather | bytes 20480 | tf_op jit(solution)/shard_map/all_gather | solution.py:29
  21.1 27.8 %all-gather.1 = bf16[64,4,512]{2,1,0:T(4,128)(2,1)S(1)} all-gather(bf16[4,4,512]{2,1,0:T(4,128)(2,1)S(1)} %all-gather.5), channel_id=3, replica_groups=mesh['ep_0'=16,'ep_1'=4,'ep_2'=2,'tp'=4] {'ep_0'}, dimensions={0}, use_global_device_ids=true | all-gather | bytes 278528 | tf_op jit(solution)/shard_map/all_gather | solution.py:29
  48.9 14.3 %all-gather.2 = bf16[32,4,4,512]{3,2,1,0:T(4,128)(2,1)S(1)} all-gather(bf16[16,4,4,512]{3,2,1,0:T(4,128)(2,1)S(1)} %bitcast.72), channel_id=4, replica_groups=mesh['ep_0'=16,'ep_1'=4,'ep_2'=2,'tp'=4] {'ep_2'}, dimensions={0}, use_global_device_ids=true | all-gather | bytes 786432 | tf_op jit(solution)/shard_map/all_gather | solution.py:29
  64.8 1.0 reshape.152
  65.7 12.0 %all-to-all-start = ((f32[128,1,192]{2,1,0:T(1,128)}), f32[128,1,192]{2,1,0:T(1,128)S(1)}, u32[]{:S(2)}, u32[]{:S(2)}) async-start(f32[128,1,192]{2,1,0:T(1,128)} %reshape.152), calls=%async_computation | async-start | bytes 262144 | tf_op jit(solution)/shard_map/all_to_all | solution.py:89
  77.9 17.0 %all-to-all-done = f32[128,1,192]{2,1,0:T(1,128)S(1)} async-done(((f32[128,1,192]{2,1,0:T(1,128)}), f32[128,1,192]{2,1,0:T(1,128)S(1)}, u32[]{:S(2)}, u32[]{:S(2)}) %all-to-all-start) | async-done | bytes 98336 | tf_op jit(solution)/shard_map/all_to_all | solution.py:89
  95.3 1.0 reduce.10
  97.4 3.3 %all-to-all-start.1 = ((f32[4,4,1536]{2,1,0:T(4,128)}), f32[4,4,1536]{2,1,0:T(4,128)S(1)}, u32[]{:S(2)}, u32[]{:S(2)}) async-start(f32[4,4,1536]{2,1,0:T(4,128)} %copy.132), calls=%async_computation.1 | async-start | bytes 196608 | tf_op jit(solution)/shard_map/all_to_all | solution.py:47
  100.9 4.4 %all-to-all-done.1 = f32[4,4,1536]{2,1,0:T(4,128)S(1)} async-done(((f32[4,4,1536]{2,1,0:T(4,128)}), f32[4,4,1536]{2,1,0:T(4,128)S(1)}, u32[]{:S(2)}, u32[]{:S(2)}) %all-to-all-start.1) | async-done | bytes 98336 | tf_op jit(solution)/shard_map/all_to_all | solution.py:47
  107.1 1.0 copy-done.1
  108.1 1.0 fusion.38
  109.2 9.1 %all_gather.40 = bf16[4,4,512]{2,1,0:T(4,128)(2,1)S(1)} all-gather(bf16[1,4,512]{2,1,0:T(4,128)(2,1)S(1)} %convert_element_type.80), channel_id=1, replica_groups=mesh['ep_0'=16,'ep_1'=4,'ep_2'=2,'tp'=4] {'ep_1'}, dimensions={0}, use_global_device_ids=true | all-gather | bytes 20480 | tf_op jit(solution)/shard_map/all_gather | solution.py:29
  118.4 20.2 %all-gather.3 = bf16[64,4,512]{2,1,0:T(4,128)(2,1)S(1)} all-gather(bf16[4,4,512]{2,1,0:T(4,128)(2,1)S(1)} %all_gather.40), channel_id=5, replica_groups=mesh['ep_0'=16,'ep_1'=4,'ep_2'=2,'tp'=4] {'ep_0'}, dimensions={0}, use_global_device_ids=true | all-gather | bytes 278528 | tf_op jit(solution)/shard_map/all_gather | solution.py:29
  138.6 13.3 %all-gather.4 = bf16[32,4,4,512]{3,2,1,0:T(4,128)(2,1)S(1)} all-gather(bf16[16,4,4,512]{3,2,1,0:T(4,128)(2,1)S(1)} %bitcast.73), channel_id=6, replica_groups=mesh['ep_0'=16,'ep_1'=4,'ep_2'=2,'tp'=4] {'ep_2'}, dimensions={0}, use_global_device_ids=true | all-gather | bytes 786432 | tf_op jit(solution)/shard_map/all_gather | solution.py:29
  153.1 0.8 copy.137
  153.9 9.0 %all-to-all-start.2 = ((bf16[128,4,16]{2,1,0:T(4,128)(2,1)}), bf16[128,4,16]{2,1,0:T(4,128)(2,1)S(1)}, u32[]{:S(2)}, u32[]{:S(2)}) async-start(bf16[128,4,16]{2,1,0:T(4,128)(2,1)} %bitcast.15), calls=%async_computation.2 | async-start | bytes 262144 | tf_op jit(solution)/shard_map/all_to_all | solution.py:111
  162.9 17.1 %all-to-all-done.2 = bf16[128,4,16]{2,1,0:T(4,128)(2,1)S(1)} async-done(((bf16[128,4,16]{2,1,0:T(4,128)(2,1)}), bf16[128,4,16]{2,1,0:T(4,128)(2,1)S(1)}, u32[]{:S(2)}, u32[]{:S(2)}) %all-to-all-start.2) | async-done | bytes 16416 | tf_op jit(solution)/shard_map/all_to_all | solution.py:111
  180.8 3.2 %all-to-all-start.3 = ((bf16[4,4,512]{2,1,0:T(4,128)(2,1)}), bf16[4,4,512]{2,1,0:T(4,128)(2,1)S(1)}, u32[]{:S(2)}, u32[]{:S(2)}) async-start(bf16[4,4,512]{2,1,0:T(4,128)(2,1)} %copy.139), calls=%async_computation.3 | async-start | bytes 32768 | tf_op jit(solution)/shard_map/all_to_all | solution.py:53
  184.2 4.1 %all-to-all-done.3 = bf16[4,4,512]{2,1,0:T(4,128)(2,1)S(1)} async-done(((bf16[4,4,512]{2,1,0:T(4,128)(2,1)}), bf16[4,4,512]{2,1,0:T(4,128)(2,1)S(1)}, u32[]{:S(2)}, u32[]{:S(2)}) %all-to-all-start.3) | async-done | bytes 16416 | tf_op jit(solution)/shard_map/all_to_all | solution.py:53
  188.4 6.9 %psum.15 = f32[4]{0:T(128)S(1)} all-reduce(f32[4]{0:T(128)S(1)} %fusion.26), channel_id=1, replica_groups=mesh['ep_0'=16,'ep_1'=4,'ep_2'=2,'tp'=4] {'tp'}, use_global_device_ids=true, to_apply=%region_9.10 | all-reduce | flops 4 | bytes 32 | tf_op jit(solution)/shard_map/psum | solution.py:129
  195.9 31.8 %all_to_all.59 = bf16[128,2,512]{2,1,0:T(2,128)(2,1)S(1)} all-to-all(bf16[128,2,512]{2,1,0:T(2,128)(2,1)S(1)} %copy.140), channel_id=1, replica_groups=mesh['ep_0'=16,'ep_1'=4,'ep_2'=2,'tp'=4] {'ep_0','ep_1','ep_2'}, dimensions={0} | all-to-all | bytes 524288 | tf_op jit(solution)/shard_map/all_to_all | solution.py:136
  228.6 17.3 %all_to_all.60 = bf16[128,2,2048]{0,1,2:T(2,128)(2,1)S(1)} all-to-all(bf16[128,2,2048]{0,1,2:T(2,128)(2,1)S(1)} %bitcast.68), channel_id=1, replica_groups=mesh['ep_0'=16,'ep_1'=4,'ep_2'=2,'tp'=4] {'tp'}, dimensions={2} | all-to-all | bytes 2097152 | tf_op jit(solution)/shard_map/all_to_all | solution.py:15
  245.9 3.0 %copy.142 = bf16[128,2,2048]{2,1,0:T(2,128)(2,1)S(1)} copy(bf16[128,2,2048]{0,1,2:T(2,128)(2,1)S(1)} %all_to_all.60) | data formatting | bytes 2097152 | tf_op jit(solution)/shard_map/all_to_all | solution.py:15
  249.4 1.5 fusion.6
  251.0 1.4 convolution_convert_fusion
  252.5 16.4 %all_to_all.61 = bf16[4,256,512]{2,1,0:T(8,128)(2,1)S(1)} all-to-all(bf16[4,256,512]{2,1,0:T(8,128)(2,1)S(1)} %bitcast.69), channel_id=1, replica_groups=mesh['ep_0'=16,'ep_1'=4,'ep_2'=2,'tp'=4] {'tp'}, dimensions={0} | all-to-all | bytes 2097152 | tf_op jit(solution)/shard_map/all_to_all | solution.py:53
  269.3 29.9 %all_to_all.62 = bf16[128,2,512]{2,1,0:T(2,128)(2,1)S(1)} all-to-all(bf16[128,2,512]{2,1,0:T(2,128)(2,1)S(1)} %convert_element_type.93), channel_id=1, replica_groups=mesh['ep_0'=16,'ep_1'=4,'ep_2'=2,'tp'=4] {'ep_0','ep_1','ep_2'}, dimensions={0} | all-to-all | bytes 524288 | tf_op jit(solution)/shard_map/all_to_all | solution.py:144
  299.2 0.8 fusion.2
  (81 shorter events, 9.9 us)
Async XLA Ops:
  0.6 250.3 %copy-start = (bf16[1,112,2048]{2,1,0:T(8,128)(2,1)S(1)}, bf16[1,112,2048]{2,1,0:T(8,128)(2,1)}, u32[]{:S(2)}) copy-start(bf16[1,112,2048]{2,1,0:T(8,128)(2,1)} %param.29) | copy-start | bytes 1376260
  63.5 0.8 copy-start.6
  63.5 0.8 copy-start.7
  63.5 0.8 copy-start.8
  64.3 13.4 %copy-start.9 = (s32[4,2]{0,1:T(2,128)S(1)}, s32[4,2]{0,1:T(2,128)}, u32[]{:S(2)}) copy-start(s32[4,2]{0,1:T(2,128)} %param.25) | copy-start | bytes 100
  64.3 13.5 %copy-start.13 = (bf16[128]{0:T(256)(128)(2,1)S(1)}, bf16[128]{0:T(256)(128)(2,1)}, u32[]{:S(2)}) copy-start(bf16[128]{0:T(256)(128)(2,1)} %param.21) | copy-start | bytes 772
  64.3 13.5 %copy-start.10 = (f32[512]{0:T(512)S(1)}, f32[512]{0:T(512)}, u32[]{:S(2)}) copy-start(f32[512]{0:T(512)} %param.20) | copy-start | bytes 6148
  65.7 29.1 %all-to-all-start = ((f32[128,1,192]{2,1,0:T(1,128)}), f32[128,1,192]{2,1,0:T(1,128)S(1)}, u32[]{:S(2)}, u32[]{:S(2)}) async-start(f32[128,1,192]{2,1,0:T(1,128)} %reshape.152), calls=%async_computation | async-start | bytes 262144 | tf_op jit(solution)/shard_map/all_to_all | solution.py:89
  96.5 10.0 %copy-start.2 = (f32[4,4,128,128]{3,2,1,0:T(8,128)S(1)}, f32[4,4,128,128]{3,2,1,0:T(8,128)}, u32[]{:S(2)}) copy-start(f32[4,4,128,128]{3,2,1,0:T(8,128)} %param.23) | copy-start | bytes 3145732
  97.4 7.9 %all-to-all-start.1 = ((f32[4,4,1536]{2,1,0:T(4,128)}), f32[4,4,1536]{2,1,0:T(4,128)S(1)}, u32[]{:S(2)}, u32[]{:S(2)}) async-start(f32[4,4,1536]{2,1,0:T(4,128)} %copy.132), calls=%async_computation.1 | async-start | bytes 196608 | tf_op jit(solution)/shard_map/all_to_all | solution.py:47
  107.1 1.0 copy-start.1
  152.2 0.7 copy-start.5
  152.6 31.5 %copy-start.11 = (f32[4,2]{0,1:T(2,128)S(1)}, f32[4,2]{0,1:T(2,128)}, u32[]{:S(2)}) copy-start(f32[4,2]{0,1:T(2,128)} %param.26) | copy-start | bytes 100
  152.6 35.6 %copy-start.4 = (bf16[4,512]{1,0:T(4,128)(2,1)S(1)}, bf16[4,512]{1,0:T(4,128)(2,1)}, u32[]{:S(2)}) copy-start(bf16[4,512]{1,0:T(4,128)(2,1)} %param.15) | copy-start | bytes 12292
  152.6 35.8 %copy-start.12 = (bf16[512]{0:T(512)(128)(2,1)S(1)}, bf16[512]{0:T(512)(128)(2,1)}, u32[]{:S(2)}) copy-start(bf16[512]{0:T(512)(128)(2,1)} %param.24) | copy-start | bytes 3076
  153.9 26.1 %all-to-all-start.2 = ((bf16[128,4,16]{2,1,0:T(4,128)(2,1)}), bf16[128,4,16]{2,1,0:T(4,128)(2,1)S(1)}, u32[]{:S(2)}, u32[]{:S(2)}) async-start(bf16[128,4,16]{2,1,0:T(4,128)(2,1)} %bitcast.15), calls=%async_computation.2 | async-start | bytes 262144 | tf_op jit(solution)/shard_map/all_to_all | solution.py:111
  180.8 7.4 %all-to-all-start.3 = ((bf16[4,4,512]{2,1,0:T(4,128)(2,1)}), bf16[4,4,512]{2,1,0:T(4,128)(2,1)S(1)}, u32[]{:S(2)}, u32[]{:S(2)}) async-start(bf16[4,4,512]{2,1,0:T(4,128)(2,1)} %copy.139), calls=%async_computation.3 | async-start | bytes 32768 | tf_op jit(solution)/shard_map/all_to_all | solution.py:53
  249.4 1.6 copy-start.3
